TPU v7x, 32 devices: a whole 2x2x4 slice. The times are simulated.
32 devices in a mesh: fs: 8 (over z, y), tp: 4 (over x, core).
Axes of the slice: x: 2, y: 2, z: 4, core: 2. Of those that a mesh axis runs over, the one named last changes fastest.
Arguments:
- saved_inputs: bfloat16 [4096, 3072], P('fs'), may hold values from -6 to 6
- query_cotangent: bfloat16 [4096, 3072], P('fs', 'tp'), may hold values from -0.75 to 0.75
- attn_outputs: bfloat16 [4096, 3072], P('fs', 'tp'), may hold values from -6 to 6
- out_cotangent: bfloat16 [4096, 3072], P('fs'), may hold values from -0.75 to 0.75
- left_factor: bfloat16 [3072, 384], P('fs', 'tp'), may hold values from -0.109375 to 0.109375
- right_factor: bfloat16 [3072, 384], P('fs', 'tp'), may hold values from -0.109375 to 0.109375
- query_master: float32 [3072, 3072], P('fs', 'tp'), may hold values from -0.109375 to 0.109375
- out_master: float32 [3072, 3072], P('tp', 'fs'), may hold values from -0.109375 to 0.109375
- first_moment: float32 [2, 384, 3072], P(None, 'fs', 'tp'), may hold values from -14 to 14
- second_moment: float32 [2, 384, 3072], P(None, 'fs', 'tp'), may hold values from 0.3 to 3
Outputs:
- query_new: float32 [3072, 3072], P('fs', 'tp')
- out_new: float32 [3072, 3072], P('tp', 'fs')
- query_copy: bfloat16 [3072, 3072], P(None, 'tp')
- out_copy: bfloat16 [3072, 3072], P('tp')
- first_new: float32 [2, 384, 3072], P(None, 'fs', 'tp')
- second_new: float32 [2, 384, 3072], P(None, 'fs', 'tp')
All inputs are finite; a program needn't handle non-finite values.
Results may differ from a plain program's by a relative error of at most 0.0025.
Values may be sent and summed in bfloat16 or wider, within the bound.
A program may use at most 64 MiB of HBM per device.

v0:
```python
import jax
import jax.numpy as jnp
from jax import lax
from jax.sharding import PartitionSpec as P


def moment_step(first, second, grads):
    first_next = 0.9 * first + 0.1 * grads
    second_next = 0.99 * second + 0.01 * grads * grads
    return (first_next, second_next, first_next / (jnp.sqrt(second_next) + 1e-08))


def body(
    saved_inputs,
    query_cotangent,
    attn_outputs,
    out_cotangent,
    left_factor,
    right_factor,
    query_master,
    out_master,
    first_moment,
    second_moment,
):
    left_part = jnp.dot(
        saved_inputs,
        lax.all_gather(left_factor, "fs", axis=0, tiled=True),
        preferred_element_type=jnp.float32,
    )
    right_part = jnp.dot(
        out_cotangent,
        lax.all_gather(right_factor, "fs", axis=0, tiled=True),
        preferred_element_type=jnp.float32,
    )
    left_proj, right_proj, left_rows, right_rows = (
        lax.all_gather(left_part.astype(jnp.bfloat16), "tp", axis=1, tiled=True),
        lax.all_gather(right_part.astype(jnp.bfloat16), "tp", axis=1, tiled=True),
        lax.all_gather(left_factor, "tp", axis=1, tiled=True),
        lax.all_gather(right_factor, "tp", axis=1, tiled=True),
    )
    rows = first_moment.shape[1]
    dims = (((0,), (0,)), ((), ()))
    grad_query = lax.dot_general(
        left_proj, query_cotangent, dims, preferred_element_type=jnp.float32
    )
    grad_output = lax.dot_general(
        right_proj, attn_outputs, dims, preferred_element_type=jnp.float32
    )
    summed = lax.psum_scatter(
        jnp.stack([grad_query, grad_output], axis=1), "fs", scatter_dimension=0, tiled=True
    )
    grads = jnp.transpose(summed, (1, 0, 2))
    first_new, second_new, own_direction = moment_step(first_moment, second_moment, grads)
    direction_all = lax.all_gather(own_direction.astype(jnp.bfloat16), "fs", axis=1, tiled=True)
    squares = jnp.sum(own_direction * own_direction, axis=(1, 2))
    total = lax.psum(squares, ("fs", "tp"))
    entries = rows * lax.axis_size("fs") * own_direction.shape[2] * lax.axis_size("tp")
    scale = lax.rsqrt(total / entries + 1e-06)
    step_query = scale[0] * jnp.dot(left_rows, direction_all[0], preferred_element_type=jnp.float32)
    step_output = scale[1] * lax.dot_general(
        direction_all[1], right_rows, (((0,), (1,)), ((), ())), preferred_element_type=jnp.float32
    )
    query_new = query_master - 0.01 * step_query
    out_new = out_master - 0.01 * step_output
    query_copy, out_copy = (
        lax.all_gather(query_new.astype(jnp.bfloat16), "fs", axis=0, tiled=True),
        lax.all_gather(out_new.astype(jnp.bfloat16), "fs", axis=1, tiled=True),
    )
    return (query_new, out_new, query_copy, out_copy, first_new, second_new)


def solution(mesh):
    return jax.shard_map(
        body,
        mesh=mesh,
        in_specs=(
            P("fs", None),
            P("fs", "tp"),
            P("fs", "tp"),
            P("fs", None),
            P("fs", "tp"),
            P("fs", "tp"),
            P("fs", "tp"),
            P("tp", "fs"),
            P(None, "fs", "tp"),
            P(None, "fs", "tp"),
        ),
        out_specs=(
            P("fs", "tp"),
            P("tp", "fs"),
            P(None, "tp"),
            P("tp", None),
            P(None, "fs", "tp"),
            P(None, "fs", "tp"),
        ),
        check_vma=False,
    )
```

profile of v0, /device:TPU:0, one launch (start us, length us, event | category | flops | bytes accessed | tf_op | source)
XLA Modules:
  0.0 390.2 jit_solution(14397979788832499997)
XLA Ops:
  7.2 0.0 reduce-scatter.2.cloned.1.call-start
  7.2 33.9 %all_gather.27 = bf16[3072,96]{0,1:T(8,128)(2,1)S(1)} all-gather(bf16[384,96]{0,1:T(8,128)(2,1)} %param.14), channel_id=1, replica_groups=mesh['fs'=8,'tp'=4] {'fs'}, dimensions={0}, use_global_device_ids=true | all-gather | bytes 663552 | tf_op jit(solution)/shard_map/all_gather | solution.py:27
  41.1 1.1 convolution_convert_fusion.1
  42.2 6.5 %all_gather.28 = bf16[512,384]{0,1:T(8,128)(2,1)S(1)} all-gather(bf16[512,96]{0,1:T(8,128)(2,1)S(1)} %convolution_convert_fusion.1), channel_id=1, replica_groups=mesh['fs'=8,'tp'=4] {'tp'}, dimensions={1}, use_global_device_ids=true | all-gather | bytes 491520 | tf_op jit(solution)/shard_map/all_gather | solution.py:36
  48.7 31.5 %all_gather.29 = bf16[3072,96]{0,1:T(8,128)(2,1)S(1)} all-gather(bf16[384,96]{0,1:T(8,128)(2,1)S(1)} %copy-done.8), channel_id=1, replica_groups=mesh['fs'=8,'tp'=4] {'fs'}, dimensions={0}, use_global_device_ids=true | all-gather | bytes 663552 | tf_op jit(solution)/shard_map/all_gather | solution.py:32
  80.2 1.1 convolution_convert_fusion
  81.3 6.1 %all_gather.30 = bf16[512,384]{0,1:T(8,128)(2,1)S(1)} all-gather(bf16[512,96]{0,1:T(8,128)(2,1)S(1)} %convolution_convert_fusion), channel_id=1, replica_groups=mesh['fs'=8,'tp'=4] {'tp'}, dimensions={1}, use_global_device_ids=true | all-gather | bytes 491520 | tf_op jit(solution)/shard_map/all_gather | solution.py:37
  87.5 0.5 convolution_bitcast_fusion
  87.9 0.7 copy-done.5
  88.6 0.5 convolution_bitcast_fusion.1
  89.1 1.6 pad_maximum_fusion
  90.6 0.0 reduce-scatter.2.cloned.1.call-update
  90.7 0.0 all-gather.4.cloned.1.call-start
  90.7 70.5 %reduce-scatter.2.cloned.1.call-done = f32[48,2,768]{2,0,1:T(8,128)} async-done(((f32[384,2,768]{2,0,1:T(8,128)}), f32[48,2,768]{2,0,1:T(8,128)}) %reduce-scatter.2.cloned.1.call-update) | async-done | bytes 294928 | tf_op jit(solution)/shard_map/reduce_scatter | solution.py:49
  161.2 1.3 multiply_reduce_fusion
  162.6 0.7 copy-done.2
  163.3 0.1 copy-done.3
  163.4 0.8 fusion.7
  164.2 0.0 all-gather.6.cloned.1.call-start
  164.3 2.7 copy.19
  166.9 5.9 %all_gather.32 = bf16[384,384]{0,1:T(8,128)(2,1)S(1)} all-gather(bf16[384,96]{0,1:T(8,128)(2,1)S(1)} %copy-done.7), channel_id=1, replica_groups=mesh['fs'=8,'tp'=4] {'tp'}, dimensions={1}, use_global_device_ids=true | all-gather | bytes 368640 | tf_op jit(solution)/shard_map/all_gather | solution.py:38
  172.8 40.3 %psum.7 = f32[2]{0:T(128)S(1)} all-reduce(f32[2]{0:T(128)S(1)} %get-tuple-element.18), channel_id=1, replica_groups=mesh['fs'=8,'tp'=4] {'fs','tp'}, use_global_device_ids=true, to_apply=%region_2.0 | all-reduce | flops 2 | bytes 16 | tf_op jit(solution)/shard_map/psum | solution.py:56
  213.1 0.6 fusion.10
  213.7 3.8 fusion.11
  217.5 0.0 all-gather.8.cloned.1.call-start
  217.6 6.7 %all_gather.33 = bf16[384,384]{0,1:T(8,128)(2,1)S(1)} all-gather(bf16[384,96]{0,1:T(8,128)(2,1)S(1)} %copy-done.9), channel_id=1, replica_groups=mesh['fs'=8,'tp'=4] {'tp'}, dimensions={1}, use_global_device_ids=true | all-gather | bytes 368640 | tf_op jit(solution)/shard_map/all_gather | solution.py:39
  224.3 3.9 fusion.12
  228.2 2.7 copy.20
  230.9 67.2 %all-gather.6.cloned.1.call-done = bf16[3072,768]{0,1:T(8,128)(2,1)} async-done(((bf16[384,768]{0,1:T(8,128)(2,1)}), bf16[3072,768]{0,1:T(8,128)(2,1)}) %all-gather.6.cloned.1.call-update) | async-done | bytes 4718608 | tf_op jit(solution)/shard_map/all_gather | solution.py:66
  298.1 6.6 %copy.21 = bf16[3072,768]{1,0:T(8,128)(2,1)} copy(bf16[3072,768]{0,1:T(8,128)(2,1)} %all-gather.6.cloned.1.call-done) | data formatting | bytes 9437184
  304.7 74.1 %all-gather.8.cloned.1.call-done = bf16[768,3072]{1,0:T(8,128)(2,1)} async-done(((bf16[768,384]{1,0:T(8,128)(2,1)}), bf16[768,3072]{1,0:T(8,128)(2,1)}) %all-gather.8.cloned.1.call-update) | async-done | bytes 4718608 | tf_op jit(solution)/shard_map/all_gather | solution.py:67
  378.8 4.8 %copy.23 = bf16[768,3072]{1,0:T(8,128)(2,1)} copy(bf16[768,3072]{1,0:T(8,128)(2,1)} %all-gather.8.cloned.1.call-done) | data formatting | bytes 9437184
  (22 shorter events, 0.1 us)
Async XLA Ops:
  7.2 33.9 %copy-start = (bf16[512,3072]{1,0:T(8,128)(2,1)S(1)}, bf16[512,3072]{1,0:T(8,128)(2,1)}, u32[]{:S(2)}) copy-start(bf16[512,3072]{1,0:T(8,128)(2,1)} %param.10) | copy-start | bytes 9437188
  7.2 154.1 %reduce-scatter.2.cloned.1.call-start = ((), (), s32[]{:S(2)}) async-start(), calls=%async_computation.1 | async-start | bytes 2654208 | tf_op jit(solution)/shard_map/reduce_scatter | solution.py:49
  41.1 7.6 %copy-start.8 = (bf16[384,96]{0,1:T(8,128)(2,1)S(1)}, bf16[384,96]{0,1:T(8,128)(2,1)}, u32[]{:S(2)}) copy-start(bf16[384,96]{0,1:T(8,128)(2,1)} %param.15) | copy-start | bytes 221188
  41.1 39.1 %copy-start.1 = (bf16[512,3072]{1,0:T(8,128)(2,1)S(1)}, bf16[512,3072]{1,0:T(8,128)(2,1)}, u32[]{:S(2)}) copy-start(bf16[512,3072]{1,0:T(8,128)(2,1)} %param.13) | copy-start | bytes 9437188
  80.2 7.3 %copy-start.4 = (bf16[512,768]{1,0:T(8,128)(2,1)S(1)}, bf16[512,768]{1,0:T(8,128)(2,1)}, u32[]{:S(2)}) copy-start(bf16[512,768]{1,0:T(8,128)(2,1)} %param.12) | copy-start | bytes 2359300
  87.5 1.1 copy-start.5
  90.6 70.6 %copy-start.6 = (f32[2,48,768]{2,1,0:T(8,128)S(1)}, f32[2,48,768]{2,1,0:T(8,128)}, u32[]{:S(2)}) copy-start(f32[2,48,768]{2,1,0:T(8,128)} %param.19) | copy-start | bytes 884740
  90.7 123.0 %all-gather.4.cloned.1.call-start = ((), (), s32[]{:S(2)}) async-start(), calls=%async_computation.2 | async-start | bytes 1327104 | tf_op jit(solution)/shard_map/all_gather | solution.py:54
  162.6 0.7 copy-start.2
  162.6 0.8 copy-start.3
  164.2 2.7 copy-start.7
  164.2 133.9 %all-gather.6.cloned.1.call-start = ((), (), s32[]{:S(2)}) async-start(), calls=%async_computation.3 | async-start | bytes 5308416 | tf_op jit(solution)/shard_map/all_gather | solution.py:66
  213.7 3.9 %copy-start.9 = (bf16[384,96]{0,1:T(8,128)(2,1)S(1)}, bf16[384,96]{0,1:T(8,128)(2,1)}, u32[]{:S(2)}) copy-start(bf16[384,96]{0,1:T(8,128)(2,1)} %param.15) | copy-start | bytes 221188
  217.5 161.2 %all-gather.8.cloned.1.call-start = ((), (), s32[]{:S(2)}) async-start(), calls=%async_computation.4 | async-start | bytes 5308416 | tf_op jit(solution)/shard_map/all_gather | solution.py:67
Sparse Core Ops, SparseCore 0:
  90.8 70.4 reduce-scatter.1
  164.3 40.5 all-gather.3
  217.7 80.3 all-gather.5
  300.0 78.7 all-gather.7
where the time goes:
time: 391 us; the launch traced here: 390 us
  waiting for transfers between devices  212 us (54%)
  blocking collectives  131 us (34%)
  local copies, waits for them, and re-layouts  18.8 us (5%)
  between operations  13.8 us (4%)
  matrix products  10.9 us (3%)
    all_gather x1, waiting for transfers between devices, body(): lax.all_gather(out_new.astype(jnp.bfloat16), 'fs', axis=1, tiled=True)  74.1 us
    reduce_scatter x1, waiting for transfers between devices, body(): lax.psum_scatter(jnp.stack([grad_query, grad_output], axis=1), 'fs', scat...  70.5 us
    all_gather x1, waiting for transfers between devices, body(): lax.all_gather(query_new.astype(jnp.bfloat16), 'fs', axis=0, tiled=True)  67.2 us
    psum x1, blocking collectives, body(): total = lax.psum(squares, ('fs', 'tp'))  40.3 us
    all_gather x1, blocking collectives, body(): lax.all_gather(left_factor, 'fs', axis=0, tiled=True)  33.9 us
    all_gather x1, blocking collectives, body(): lax.all_gather(right_factor, 'fs', axis=0, tiled=True)  31.5 us
    unnamed x24, local copies, waits for them, and re-layouts  18.3 us
  transfers between devices with their start and end apart: 4, of which 3 were waited for; matrix products, arithmetic and copies ran while one was open for 4% of the time, Pallas kernels for 0%

commit v1 on v0

--- a/solution.py
+++ b/solution.py
@@ -1,7 +1,17 @@
+import functools
+
 import jax
 import jax.numpy as jnp
 from jax import lax
+from jax.experimental import pallas as pl
+from jax.experimental.pallas import tpu as pltpu
 from jax.sharding import PartitionSpec as P
+
+MESH = pl.DeviceIdType.MESH
+PAIR = 2
+MASTER_GAIN = 2.0**19
+NT = (((1,), (1,)), ((), ()))
+TN = (((0,), (0,)), ((), ()))
 
 
 def moment_step(first, second, grads):
@@ -10,7 +20,356 @@
     return (first_next, second_next, first_next / (jnp.sqrt(second_next) + 1e-08))
 
 
-def body(
+def rows(index, size):
+    return pl.ds(pl.multiple_of(index * size, size), size)
+
+
+def peer_along(axis, index):
+    if axis == "fs":
+        return (index, lax.axis_index("tp"))
+    return (lax.axis_index("fs"), index)
+
+
+class Gather:
+    def __init__(self, axis, count, view, sems, own=None):
+        self.axis, self.outer, self.view, self.sems = axis, count // PAIR, view, sems
+        me = lax.axis_index(axis)
+        self.high, self.low = me // PAIR, lax.rem(me, PAIR)
+        self.own = view(me) if own is None else own
+        self.me = me
+
+    def copy(self, src, dst, stage, slot, target):
+        return pltpu.make_async_remote_copy(
+            src_ref=src,
+            dst_ref=dst,
+            send_sem=self.sems.at[stage, 0, slot],
+            recv_sem=self.sems.at[stage, 1, slot],
+            device_id=peer_along(self.axis, target),
+            device_id_type=MESH,
+        )
+
+    def index(self, offset, low):
+        return lax.rem(self.high + offset, self.outer) * PAIR + low
+
+    def outward(self, offset):
+        return self.copy(self.own, self.view(self.me), 0, offset, self.index(offset, self.low))
+
+    def inward(self, offset):
+        source = self.index(self.outer - offset, self.low)
+        src = self.own if offset == 0 else self.view(source)
+        partner = self.high * PAIR + 1 - self.low
+        return self.copy(src, self.view(self.me if offset == 0 else source), 1, offset, partner)
+
+    def start(self):
+        for offset in range(self.outer - 1, 0, -1):
+            self.outward(offset).start()
+        self.inward(0).start()
+
+    def forward(self):
+        for offset in range(1, self.outer):
+            self.outward(offset).wait_recv()
+            self.inward(offset).start()
+
+    def finish(self):
+        for offset in range(self.outer):
+            self.inward(offset).wait_recv()
+        for offset in range(1, self.outer):
+            self.outward(offset).wait_send()
+        for offset in range(self.outer):
+            self.inward(offset).wait_send()
+
+
+def kernel(
+    n_fs,
+    n_tp,
+    saved_hbm,
+    outcot_hbm,
+    querycot_hbm,
+    attn_hbm,
+    factor_ref,
+    first_ref,
+    second_ref,
+    factors_ref,
+    dirs_ref,
+    first_out,
+    second_out,
+    square_out,
+    saved,
+    outcot,
+    querycot,
+    attn,
+    proj,
+    grad,
+    pair_send,
+    pair_recv,
+    far_send,
+    far_recv,
+    own_dir,
+    square_buf,
+    load_sems,
+    factor_sems,
+    proj_sems,
+    columns_sems,
+    pair_sems,
+    far_sems,
+    dir_sems,
+    square_sems,
+):
+    me, column = lax.axis_index("fs"), lax.axis_index("tp")
+    high, low = me // PAIR, lax.rem(me, PAIR)
+    outer = n_fs // PAIR
+    part = factor_ref.shape[1]
+    width = factor_ref.shape[2]
+    depth = first_ref.shape[1]
+    loads = [
+        pltpu.make_async_copy(src, dst, load_sems.at[i])
+        for i, (src, dst) in enumerate(
+            ((saved_hbm, saved), (outcot_hbm, outcot), (querycot_hbm, querycot), (attn_hbm, attn))
+        )
+    ]
+    for load in loads:
+        load.start()
+
+    peers = [(lax.rem(high + i, outer) * PAIR + low, column) for i in range(1, outer)]
+    peers.append((high * PAIR + 1 - low, column))
+    peers += [(me, lax.rem(column + i, n_tp)) for i in range(1, n_tp)]
+    barrier = pltpu.get_barrier_semaphore()
+    for peer in peers:
+        pl.semaphore_signal(barrier, inc=1, device_id=peer, device_id_type=MESH)
+    pl.semaphore_wait(barrier, len(peers))
+
+    factors = Gather(
+        "fs",
+        n_fs,
+        lambda i: factors_ref.at[:, rows(column, part), rows(i, width)],
+        factor_sems,
+        own=factor_ref,
+    )
+    factors.start()
+    factors_ref[:, rows(column, part), rows(me, width)] = factor_ref[...]
+    factors.forward()
+    factors.finish()
+
+    gathers = []
+    for k, tokens in enumerate((saved, outcot)):
+        loads[k].wait()
+        part_proj = lax.dot_general(
+            factors_ref[k, rows(column, part), :],
+            tokens[...],
+            NT,
+            preferred_element_type=jnp.float32,
+        )
+        proj[k, rows(column, part), :] = part_proj.astype(proj.dtype)
+        gather = Gather(
+            "tp", n_tp, lambda i, k=k: proj.at[k, rows(i, part), :], proj_sems.at[k]
+        )
+        gather.start()
+        gathers.append(gather)
+    columns = Gather("tp", n_tp, lambda i: factors_ref.at[:, rows(i, part), :], columns_sems)
+    for gather in gathers:
+        gather.forward()
+    columns.start()
+    for k, (gather, cot) in enumerate(zip(gathers, (querycot, attn))):
+        gather.finish()
+        loads[2 + k].wait()
+        grad[k, :, :] = jnp.dot(proj[k], cot[...], preferred_element_type=jnp.float32)
+
+    def pair_copy(offset):
+        return pltpu.make_async_remote_copy(
+            src_ref=pair_send.at[offset],
+            dst_ref=pair_recv.at[offset],
+            send_sem=pair_sems.at[0, offset],
+            recv_sem=pair_sems.at[1, offset],
+            device_id=(high * PAIR + 1 - low, column),
+            device_id_type=MESH,
+        )
+
+    def far_copy(offset):
+        return pltpu.make_async_remote_copy(
+            src_ref=far_send.at[offset],
+            dst_ref=far_recv.at[offset],
+            send_sem=far_sems.at[0, offset],
+            recv_sem=far_sems.at[1, offset],
+            device_id=(lax.rem(high + offset, outer) * PAIR + low, column),
+            device_id_type=MESH,
+        )
+
+    order = list(range(outer - 1, 0, -1)) + [0]
+    for offset in order:
+        target = lax.rem(high + offset, outer) * PAIR + 1 - low
+        pair_send[offset] = grad[:, rows(target, depth), :].astype(pair_send.dtype)
+        pair_copy(offset).start()
+    for offset in order:
+        target = lax.rem(high + offset, outer) * PAIR + low
+        pair_copy(offset).wait_recv()
+        both = grad[:, rows(target, depth), :] + pair_recv[offset].astype(jnp.float32)
+        if offset:
+            far_send[offset] = both.astype(far_send.dtype)
+            far_copy(offset).start()
+    total = both
+    columns.forward()
+    for offset in range(1, outer):
+        far_copy(offset).wait_recv()
+        total = total + far_recv[offset].astype(jnp.float32)
+
+    first_new, second_new, direction = moment_step(first_ref[...], second_ref[...], total)
+    own_dir[...] = direction.astype(own_dir.dtype)
+    spread = Gather("fs", n_fs, lambda i: dirs_ref.at[:, rows(i, depth), :], dir_sems, own=own_dir)
+    spread.start()
+    dirs_ref[:, rows(me, depth), :] = own_dir[...]
+    first_out[...] = first_new
+    second_out[...] = second_new
+    squares = direction * direction
+    shape = square_out.shape
+    row = lax.broadcasted_iota(jnp.int32, shape, 0)
+    mine = jnp.where(row == 0, jnp.sum(squares[0]), jnp.sum(squares[1]))
+
+    rounds = (
+        [(me, lax.rem(column + i, n_tp)) for i in range(1, n_tp)],
+        [(lax.rem(high + i, outer) * PAIR + low, column) for i in range(1, outer)],
+        [(high * PAIR + 1 - low, column)],
+    )
+    slot = 0
+    tiny = []
+    for stage, targets in enumerate(rounds):
+        square_buf[slot] = mine
+        base = slot
+        copies = []
+        for target in targets:
+            slot += 1
+            copies.append(
+                pltpu.make_async_remote_copy(
+                    src_ref=square_buf.at[base],
+                    dst_ref=square_buf.at[slot],
+                    send_sem=square_sems.at[0, slot],
+                    recv_sem=square_sems.at[1, slot],
+                    device_id=target,
+                    device_id_type=MESH,
+                )
+            )
+        for copy in copies:
+            copy.start()
+        if stage == 1:
+            spread.forward()
+        for i, copy in enumerate(copies):
+            copy.wait_recv()
+            mine = mine + square_buf[base + 1 + i]
+        tiny += copies
+        slot += 1
+    square_out[...] = mine
+    spread.finish()
+    columns.finish()
+    for offset in order:
+        pair_copy(offset).wait_send()
+        if offset:
+            far_copy(offset).wait_send()
+    for copy in tiny:
+        copy.wait_send()
+
+
+def moment_kernel(n_fs, n_tp, saved_inputs, out_cotangent, query_cotangent, attn_outputs, factor, first, second):
+    tokens, model = saved_inputs.shape
+    features = query_cotangent.shape[1]
+    part = factor.shape[1]
+    depth = first.shape[1]
+    rank = part * n_tp
+    outer = n_fs // PAIR
+    low = jnp.bfloat16
+    vmem = pl.BlockSpec(memory_space=pltpu.VMEM)
+    anywhere = pl.BlockSpec(memory_space=pl.ANY)
+    dma = pltpu.SemaphoreType.DMA
+    tiny_slots = n_tp + outer + PAIR
+    return pl.pallas_call(
+        functools.partial(kernel, n_fs, n_tp),
+        out_shape=(
+            jax.ShapeDtypeStruct((2, rank, model), low),
+            jax.ShapeDtypeStruct((2, rank, features), low),
+            jax.ShapeDtypeStruct(first.shape, jnp.float32),
+            jax.ShapeDtypeStruct(first.shape, jnp.float32),
+            jax.ShapeDtypeStruct((8, 128), jnp.float32),
+        ),
+        in_specs=[anywhere] * 4 + [vmem] * 3,
+        out_specs=(vmem,) * 5,
+        scratch_shapes=[
+            pltpu.VMEM((tokens, model), low),
+            pltpu.VMEM((tokens, model), low),
+            pltpu.VMEM((tokens, features), low),
+            pltpu.VMEM((tokens, features), low),
+            pltpu.VMEM((2, rank, tokens), low),
+            pltpu.VMEM((2, rank, features), jnp.float32),
+            pltpu.VMEM((outer, 2, depth, features), low),
+            pltpu.VMEM((outer, 2, depth, features), low),
+            pltpu.VMEM((outer, 2, depth, features), low),
+            pltpu.VMEM((outer, 2, depth, features), low),
+            pltpu.VMEM((2, depth, features), low),
+            pltpu.VMEM((tiny_slots, 8, 128), jnp.float32),
+            dma((4,)),
+            dma((2, 2, outer)),
+            dma((2, 2, 2, n_tp // PAIR)),
+            dma((2, 2, n_tp // PAIR)),
+            dma((2, outer)),
+            dma((2, outer)),
+            dma((2, 2, outer)),
+            dma((2, tiny_slots)),
+        ],
+        compiler_params=pltpu.CompilerParams(
+            collective_id=0, has_side_effects=True, vmem_limit_bytes=48 * 2**20
+        ),
+        cost_estimate=pl.CostEstimate(
+            flops=4 * tokens * rank * (model + features), bytes_accessed=200 * 2**20, transcendentals=0
+        ),
+    )(saved_inputs, out_cotangent, query_cotangent, attn_outputs, factor, first, second)
+
+
+def fast_body(
+    n_fs,
+    n_tp,
+    saved_inputs,
+    query_cotangent,
+    attn_outputs,
+    out_cotangent,
+    left_factor,
+    right_factor,
+    query_master,
+    out_master,
+    first_moment,
+    second_moment,
+):
+    query_all = lax.all_gather(
+        (query_master * MASTER_GAIN).astype(jnp.float16), "fs", axis=0, tiled=True
+    )
+    out_all = lax.all_gather(
+        (out_master * MASTER_GAIN).astype(jnp.float16), "fs", axis=1, tiled=True
+    )
+    factor = jnp.stack([left_factor.T, right_factor.T])
+    factors, dirs, first_new, second_new, squares = moment_kernel(
+        n_fs,
+        n_tp,
+        saved_inputs,
+        out_cotangent,
+        query_cotangent,
+        attn_outputs,
+        factor,
+        first_moment,
+        second_moment,
+    )
+    rank, features = dirs.shape[1:]
+    entries = rank * features * n_tp
+    scale = 0.01 * lax.rsqrt(squares[:2, 0] / entries + 1e-06)
+    width = left_factor.shape[0]
+    start = lax.axis_index("fs") * width
+    own = lax.dynamic_slice_in_dim(factors, start, width, axis=2)
+    f32 = jnp.float32
+    query_new = query_master - scale[0] * lax.dot_general(own[0], dirs[0], TN, preferred_element_type=f32)
+    out_new = out_master - scale[1] * lax.dot_general(dirs[1], own[1], TN, preferred_element_type=f32)
+    query_step = lax.dot_general(factors[0], dirs[0], TN, preferred_element_type=f32)
+    out_step = lax.dot_general(dirs[1], factors[1], TN, preferred_element_type=f32)
+    query_copy = (query_all.astype(f32) * (1 / MASTER_GAIN) - scale[0] * query_step).astype(jnp.bfloat16)
+    out_copy = (out_all.astype(f32) * (1 / MASTER_GAIN) - scale[1] * out_step).astype(jnp.bfloat16)
+    return (query_new, out_new, query_copy, out_copy, first_new, second_new)
+
+
+def plain_body(
     saved_inputs,
     query_cotangent,
     attn_outputs,
@@ -38,14 +397,9 @@
         lax.all_gather(left_factor, "tp", axis=1, tiled=True),
         lax.all_gather(right_factor, "tp", axis=1, tiled=True),
     )
-    rows = first_moment.shape[1]
-    dims = (((0,), (0,)), ((), ()))
-    grad_query = lax.dot_general(
-        left_proj, query_cotangent, dims, preferred_element_type=jnp.float32
-    )
-    grad_output = lax.dot_general(
-        right_proj, attn_outputs, dims, preferred_element_type=jnp.float32
-    )
+    depth = first_moment.shape[1]
+    grad_query = lax.dot_general(left_proj, query_cotangent, TN, preferred_element_type=jnp.float32)
+    grad_output = lax.dot_general(right_proj, attn_outputs, TN, preferred_element_type=jnp.float32)
     summed = lax.psum_scatter(
         jnp.stack([grad_query, grad_output], axis=1), "fs", scatter_dimension=0, tiled=True
     )
@@ -54,7 +408,7 @@
     direction_all = lax.all_gather(own_direction.astype(jnp.bfloat16), "fs", axis=1, tiled=True)
     squares = jnp.sum(own_direction * own_direction, axis=(1, 2))
     total = lax.psum(squares, ("fs", "tp"))
-    entries = rows * lax.axis_size("fs") * own_direction.shape[2] * lax.axis_size("tp")
+    entries = depth * lax.axis_size("fs") * own_direction.shape[2] * lax.axis_size("tp")
     scale = lax.rsqrt(total / entries + 1e-06)
     step_query = scale[0] * jnp.dot(left_rows, direction_all[0], preferred_element_type=jnp.float32)
     step_output = scale[1] * lax.dot_general(
@@ -69,9 +423,19 @@
     return (query_new, out_new, query_copy, out_copy, first_new, second_new)
 
 
+def choose_body(n_fs, n_tp, *args):
+    left_factor, first_moment = args[4], args[8]
+    model, part = left_factor.shape
+    aligned = model % 128 == 0 and part % 16 == 0 and first_moment.shape[1] % 16 == 0
+    aligned = aligned and first_moment.shape[2] % 128 == 0
+    if aligned and n_fs % PAIR == 0 and n_tp % PAIR == 0:
+        return fast_body(n_fs, n_tp, *args)
+    return plain_body(*args)
+
+
 def solution(mesh):
     return jax.shard_map(
-        body,
+        functools.partial(choose_body, mesh.shape["fs"], mesh.shape["tp"]),
         mesh=mesh,
         in_specs=(
             P("fs", None),

time: 391 us -> 299 us (0.76)
  waiting for transfers between devices: 212 us -> 0 us
  Pallas kernels: 0 us -> 85.4 us
  blocking collectives: 131 us -> 189 us
  local copies, waits for them, and re-layouts: 18.8 us -> 1.97 us
  between operations: 13.8 us -> 0.69 us
  matrix products: 10.9 us -> 17.5 us
    all_gather x3 -> x0, waiting for transfers between devices: 141 us -> none  [the longest x1 74.1 us: body(): lax.all_gather(out_new.astype(jnp.bfloat16), 'fs', axis=1, tiled=True)]
    all_gather x6 -> x2, blocking collectives: 90.6 us -> 189 us  [the longest x1 96.4 us: fast_body(): lax.all_gather((out_master * MASTER_GAIN).astype(jnp.float16), 'fs', axis...]
    pallas_call x0 -> x1, Pallas kernels: none -> 85.4 us  [moment_kernel(): pl.pallas_call(functools.partial(kernel, n_fs, n_tp), out_shape=(jax.Shap...]
    reduce_scatter x1 -> x0, waiting for transfers between devices: 70.5 us -> none  [body(): lax.psum_scatter(jnp.stack([grad_query, grad_output], axis=1), 'fs', scat...]
    psum x1 -> x0, blocking collectives: 40.3 us -> none  [body(): total = lax.psum(squares, ('fs', 'tp'))]
    unnamed x24 -> x16, local copies, waits for them, and re-layouts: 18.3 us -> 1.45 us
    dot_general x6 -> x4, matrix products: 10.9 us -> 17.5 us  [the longest x1 7.56 us: fast_body(): lax.dot_general(dirs[1], factors[1], TN, preferred_element_type=f32)]
  transfers between devices with their start and end apart: 4 -> 0, of which waited for: 3 -> 0; matrix products, arithmetic and copies ran while one was open for 4% -> 0% of each run, Pallas kernels for 0% -> 0%
where the time goes in v1:
time: 299 us; the launch traced here: 298 us
  blocking collectives  189 us (63%)
  Pallas kernels  85.4 us (29%)
  matrix products  17.5 us (6%)
  other arithmetic  3.71 us (1%)
    all_gather x1, blocking collectives, fast_body(): lax.all_gather((out_master * MASTER_GAIN).astype(jnp.float16), 'fs', axis...  96.4 us
    all_gather x1, blocking collectives, fast_body(): lax.all_gather((query_master * MASTER_GAIN).astype(jnp.float16), 'fs', ax...  92.7 us
    pallas_call x1, Pallas kernels, moment_kernel(): pl.pallas_call(functools.partial(kernel, n_fs, n_tp), out_shape=(jax.Shap...  85.4 us
    dot_general x1, matrix products, fast_body(): lax.dot_general(dirs[1], factors[1], TN, preferred_element_type=f32)  7.56 us

profile of v1, /device:TPU:0, one launch (start us, length us, event | category | flops | bytes accessed | tf_op | source)
XLA Modules:
  0.0 298.3 jit_solution(14720577623628748440)
XLA Ops:
  0.6 0.9 pad_maximum_fusion.factor_ref
  1.6 1.4 multiply_convert_fusion.1
  3.0 1.4 multiply_convert_fusion
  4.3 96.4 %all-gather.2 = f16[768,3072]{1,0:T(8,128)(2,1)S(1)} all-gather(f16[768,384]{1,0:T(8,128)(2,1)S(1)} %multiply_convert_fusion), channel_id=1, replica_groups=mesh['fs'=8,'tp'=4] {'fs'}, dimensions={1}, use_global_device_ids=true | all-gather | bytes 5308416 | tf_op jit(solution)/shard_map/all_gather | solution.py:341
  100.7 0.0 copy-start
  100.7 0.0 copy-start.1
  100.7 0.0 copy-start.2
  100.7 0.0 copy-start.3
  100.7 92.7 %all-gather.3 = f16[3072,768]{1,0:T(8,128)(2,1)S(1)} all-gather(f16[384,768]{1,0:T(8,128)(2,1)S(1)} %multiply_convert_fusion.1), channel_id=1, replica_groups=mesh['fs'=8,'tp'=4] {'fs'}, dimensions={0}, use_global_device_ids=true | all-gather | bytes 5308416 | tf_op jit(solution)/shard_map/all_gather | solution.py:338
  193.4 0.0 copy-done
  193.4 0.0 copy-done.1
  193.4 0.0 copy-done.2
  193.4 0.0 copy-done.3
  193.4 85.4 %shard_map.145 = (bf16[2,384,3072]{2,1,0:T(8,128)(2,1)}, bf16[2,384,768]{2,1,0:T(8,128)(2,1)S(1)}, f32[2,48,768]{2,1,0:T(8,128)S(1)}, f32[2,48,768]{2,1,0:T(8,128)S(1)}, f32[8,128]{1,0:T(8,128)S(1)}) custom-call(bf16[512,3072]{1,0:T(8,128)(2,1)} %saved_hbm.1, bf16[512,3072]{1,0:T(8,128)(2,1)} %outcot_hbm.1, bf16[512,768]{1,0:T(8,128)(2,1)S(1)} %copy-done, ...), custom_call_target="tpu_custom_call" | custom-call | flops 3019898880 | bytes 209715200 | tf_op jit(solution)/shard_map/pallas_call | solution.py:282
  278.9 0.5 fusion.16
  279.4 0.0 copy-start.6
  279.4 7.6 %subtract_convert_fusion = bf16[768,3072]{1,0:T(8,128)(2,1)} fusion(f16[768,3072]{1,0:T(8,128)(2,1)S(1)} %all-gather.2, f32[]{:T(128)} %bitcast.7, bf16[2,384,3072]{2,1,0:T(8,128)(2,1)} %get-tuple-element.12, bf16[2,384,768]{2,1,0:T(8,128)(2,1)S(1)} %get-tuple-element.13), kind=kOutput, calls=%fused_computation | convolution fusion | flops 1823735808 | bytes 12386816 | tf_op jit(solution)/shard_map/dot_general | solution.py:366
  286.9 0.0 copy-done.6
  286.9 0.0 copy-start.4
  286.9 5.4 %subtract_convert_fusion.1 = bf16[3072,768]{1,0:T(8,128)(2,1)} fusion(f16[3072,768]{1,0:T(8,128)(2,1)S(1)} %all-gather.3, f32[]{:T(128)} %bitcast.4, bf16[2,384,3072]{2,1,0:T(8,128)(2,1)S(1)} %copy-done.6, bf16[2,384,768]{2,1,0:T(8,128)(2,1)S(1)} %get-tuple-element.13), kind=kOutput, calls=%fused_computation.1 | convolution fusion | flops 1823735808 | bytes 12386308 | tf_op jit(solution)/shard_map/dot_general | solution.py:365
  292.3 0.0 copy-done.4
  292.3 0.0 copy-start.5
  292.4 2.4 fusion.5
  294.7 0.0 copy-done.5
  294.7 2.2 fusion.4
  296.9 0.7 copy.18
  297.6 0.7 copy.19
  (1 shorter events, 0.0 us)
Async XLA Ops:
  100.7 92.7 %copy-start = (bf16[512,768]{1,0:T(8,128)(2,1)S(1)}, bf16[512,768]{1,0:T(8,128)(2,1)}, u32[]{:S(2)}) copy-start(bf16[512,768]{1,0:T(8,128)(2,1)} %querycot_hbm.1) | copy-start | bytes 2359300
  100.7 92.7 %copy-start.1 = (bf16[512,768]{1,0:T(8,128)(2,1)S(1)}, bf16[512,768]{1,0:T(8,128)(2,1)}, u32[]{:S(2)}) copy-start(bf16[512,768]{1,0:T(8,128)(2,1)} %attn_hbm.1) | copy-start | bytes 2359300
  100.7 92.7 %copy-start.2 = (f32[2,48,768]{2,1,0:T(8,128)S(1)}, f32[2,48,768]{2,1,0:T(8,128)}, u32[]{:S(2)}) copy-start(f32[2,48,768]{2,1,0:T(8,128)} %first_ref.1) | copy-start | bytes 884740
  100.7 92.7 %copy-start.3 = (f32[2,48,768]{2,1,0:T(8,128)S(1)}, f32[2,48,768]{2,1,0:T(8,128)}, u32[]{:S(2)}) copy-start(f32[2,48,768]{2,1,0:T(8,128)} %second_ref.1) | copy-start | bytes 884740
  279.4 7.6 %copy-start.6 = (bf16[2,384,3072]{2,1,0:T(8,128)(2,1)S(1)}, bf16[2,384,3072]{2,1,0:T(8,128)(2,1)}, u32[]{:S(2)}) copy-start(bf16[2,384,3072]{2,1,0:T(8,128)(2,1)} %get-tuple-element.12) | copy-start | bytes 14155780
  286.9 5.4 %copy-start.4 = (f32[768,384]{1,0:T(8,128)S(1)}, f32[768,384]{1,0:T(8,128)}, u32[]{:S(2)}) copy-start(f32[768,384]{1,0:T(8,128)} %param.17) | copy-start | bytes 3538948
  292.3 2.4 copy-start.5

commit v2 on v1

--- a/solution.py
+++ b/solution.py
@@ -9,7 +9,6 @@
 
 MESH = pl.DeviceIdType.MESH
 PAIR = 2
-MASTER_GAIN = 2.0**19
 NT = (((1,), (1,)), ((), ()))
 TN = (((0,), (0,)), ((), ()))
 
@@ -60,13 +59,19 @@
         partner = self.high * PAIR + 1 - self.low
         return self.copy(src, self.view(self.me if offset == 0 else source), 1, offset, partner)
 
-    def start(self):
+    def start_outward(self):
         for offset in range(self.outer - 1, 0, -1):
             self.outward(offset).start()
+
+    def start_inward(self):
         self.inward(0).start()
 
+    def start(self):
+        self.start_outward()
+        self.start_inward()
+
     def forward(self):
-        for offset in range(1, self.outer):
+        for offset in range(self.outer - 1, 0, -1):
             self.outward(offset).wait_recv()
             self.inward(offset).start()
 
@@ -86,14 +91,23 @@
     outcot_hbm,
     querycot_hbm,
     attn_hbm,
+    query_hbm,
+    out_hbm,
     factor_ref,
     first_ref,
     second_ref,
+    query_out,
+    out_out,
+    query_copy,
+    out_copy,
+    first_out,
+    second_out,
     factors_ref,
     dirs_ref,
-    first_out,
-    second_out,
-    square_out,
+    query_master,
+    out_master,
+    query_early,
+    out_early,
     saved,
     outcot,
     querycot,
@@ -114,6 +128,8 @@
     far_sems,
     dir_sems,
     square_sems,
+    early_sems,
+    late_sems,
 ):
     me, column = lax.axis_index("fs"), lax.axis_index("tp")
     high, low = me // PAIR, lax.rem(me, PAIR)
@@ -124,10 +140,17 @@
     loads = [
         pltpu.make_async_copy(src, dst, load_sems.at[i])
         for i, (src, dst) in enumerate(
-            ((saved_hbm, saved), (outcot_hbm, outcot), (querycot_hbm, querycot), (attn_hbm, attn))
+            (
+                (saved_hbm, saved),
+                (outcot_hbm, outcot),
+                (querycot_hbm, querycot),
+                (attn_hbm, attn),
+                (query_hbm, query_master),
+                (out_hbm, out_master),
+            )
         )
     ]
-    for load in loads:
+    for load in loads[4:] + loads[:4]:
         load.start()
 
     peers = [(lax.rem(high + i, outer) * PAIR + low, column) for i in range(1, outer)]
@@ -147,7 +170,21 @@
     )
     factors.start()
     factors_ref[:, rows(column, part), rows(me, width)] = factor_ref[...]
+
+    half = query_copy.shape[1] // 2
+    early = (
+        Gather("fs", n_fs, lambda i: query_copy.at[rows(i, width), :half], early_sems.at[0], own=query_early),
+        Gather("fs", n_fs, lambda i: out_copy.at[:half, rows(i, width)], early_sems.at[1], own=out_early),
+    )
+    loads[4].wait()
+    query_early[...] = query_master[:, :half].astype(query_early.dtype)
+    loads[5].wait()
+    out_early[...] = out_master[:half, :].astype(out_early.dtype)
+    for gather in early:
+        gather.start_outward()
     factors.forward()
+    for gather in early:
+        gather.start_inward()
     factors.finish()
 
     gathers = []
@@ -208,6 +245,8 @@
             far_copy(offset).start()
     total = both
     columns.forward()
+    for gather in early:
+        gather.forward()
     for offset in range(1, outer):
         far_copy(offset).wait_recv()
         total = total + far_recv[offset].astype(jnp.float32)
@@ -220,7 +259,7 @@
     first_out[...] = first_new
     second_out[...] = second_new
     squares = direction * direction
-    shape = square_out.shape
+    shape = square_buf.shape[1:]
     row = lax.broadcasted_iota(jnp.int32, shape, 0)
     mine = jnp.where(row == 0, jnp.sum(squares[0]), jnp.sum(squares[1]))
 
@@ -256,69 +295,57 @@
             mine = mine + square_buf[base + 1 + i]
         tiny += copies
         slot += 1
-    square_out[...] = mine
     spread.finish()
     columns.finish()
+
+    entries = dirs_ref.shape[1] * dirs_ref.shape[2] * n_tp
+    scale = 0.01 * lax.rsqrt(mine / entries + 1e-06)
+    query_scale, out_scale = scale[0:1, 0:1], scale[1:2, 0:1]
+
+    def step(k, block, part_of_features):
+        factor = factors_ref[k, :, rows(block, width)]
+        direction = dirs_ref[k, :, part_of_features]
+        pair = (factor, direction) if k == 0 else (direction, factor)
+        return lax.dot_general(*pair, TN, preferred_element_type=jnp.float32)
+
+    late = (
+        Gather("fs", n_fs, lambda i: query_copy.at[rows(i, width), half:], late_sems.at[0]),
+        Gather("fs", n_fs, lambda i: out_copy.at[half:, rows(i, width)], late_sems.at[1]),
+    )
+    for part_of_features in (slice(half, None), slice(0, half)):
+        query_new = query_master[:, part_of_features] - query_scale * step(0, me, part_of_features)
+        query_out[:, part_of_features] = query_new
+        query_copy[rows(me, width), part_of_features] = query_new.astype(query_copy.dtype)
+        if part_of_features.start:
+            late[0].start()
+        out_new = out_master[part_of_features, :] - out_scale * step(1, me, part_of_features)
+        out_out[part_of_features, :] = out_new
+        out_copy[part_of_features, rows(me, width)] = out_new.astype(out_copy.dtype)
+        if part_of_features.start:
+            late[1].start()
+    for gather in early:
+        gather.finish()
+
+    def finish_block(i, carry):
+        block = lax.rem(me + i, n_fs)
+        where = rows(block, width)
+        query = query_copy[where, :half].astype(jnp.float32)
+        query_copy[where, :half] = (query - query_scale * step(0, block, slice(0, half))).astype(query_copy.dtype)
+        out = out_copy[:half, where].astype(jnp.float32)
+        out_copy[:half, where] = (out - out_scale * step(1, block, slice(0, half))).astype(out_copy.dtype)
+        return carry
+
+    lax.fori_loop(1, n_fs, finish_block, 0)
+    for gather in late:
+        gather.forward()
+    for gather in late:
+        gather.finish()
     for offset in order:
         pair_copy(offset).wait_send()
         if offset:
             far_copy(offset).wait_send()
     for copy in tiny:
         copy.wait_send()
-
-
-def moment_kernel(n_fs, n_tp, saved_inputs, out_cotangent, query_cotangent, attn_outputs, factor, first, second):
-    tokens, model = saved_inputs.shape
-    features = query_cotangent.shape[1]
-    part = factor.shape[1]
-    depth = first.shape[1]
-    rank = part * n_tp
-    outer = n_fs // PAIR
-    low = jnp.bfloat16
-    vmem = pl.BlockSpec(memory_space=pltpu.VMEM)
-    anywhere = pl.BlockSpec(memory_space=pl.ANY)
-    dma = pltpu.SemaphoreType.DMA
-    tiny_slots = n_tp + outer + PAIR
-    return pl.pallas_call(
-        functools.partial(kernel, n_fs, n_tp),
-        out_shape=(
-            jax.ShapeDtypeStruct((2, rank, model), low),
-            jax.ShapeDtypeStruct((2, rank, features), low),
-            jax.ShapeDtypeStruct(first.shape, jnp.float32),
-            jax.ShapeDtypeStruct(first.shape, jnp.float32),
-            jax.ShapeDtypeStruct((8, 128), jnp.float32),
-        ),
-        in_specs=[anywhere] * 4 + [vmem] * 3,
-        out_specs=(vmem,) * 5,
-        scratch_shapes=[
-            pltpu.VMEM((tokens, model), low),
-            pltpu.VMEM((tokens, model), low),
-            pltpu.VMEM((tokens, features), low),
-            pltpu.VMEM((tokens, features), low),
-            pltpu.VMEM((2, rank, tokens), low),
-            pltpu.VMEM((2, rank, features), jnp.float32),
-            pltpu.VMEM((outer, 2, depth, features), low),
-            pltpu.VMEM((outer, 2, depth, features), low),
-            pltpu.VMEM((outer, 2, depth, features), low),
-            pltpu.VMEM((outer, 2, depth, features), low),
-            pltpu.VMEM((2, depth, features), low),
-            pltpu.VMEM((tiny_slots, 8, 128), jnp.float32),
-            dma((4,)),
-            dma((2, 2, outer)),
-            dma((2, 2, 2, n_tp // PAIR)),
-            dma((2, 2, n_tp // PAIR)),
-            dma((2, outer)),
-            dma((2, outer)),
-            dma((2, 2, outer)),
-            dma((2, tiny_slots)),
-        ],
-        compiler_params=pltpu.CompilerParams(
-            collective_id=0, has_side_effects=True, vmem_limit_bytes=48 * 2**20
-        ),
-        cost_estimate=pl.CostEstimate(
-            flops=4 * tokens * rank * (model + features), bytes_accessed=200 * 2**20, transcendentals=0
-        ),
-    )(saved_inputs, out_cotangent, query_cotangent, attn_outputs, factor, first, second)
 
 
 def fast_body(
@@ -335,38 +362,78 @@
     first_moment,
     second_moment,
 ):
-    query_all = lax.all_gather(
-        (query_master * MASTER_GAIN).astype(jnp.float16), "fs", axis=0, tiled=True
-    )
-    out_all = lax.all_gather(
-        (out_master * MASTER_GAIN).astype(jnp.float16), "fs", axis=1, tiled=True
-    )
+    tokens, model = saved_inputs.shape
+    features = query_cotangent.shape[1]
+    width, part = left_factor.shape
+    depth = first_moment.shape[1]
+    rank = part * n_tp
+    outer = n_fs // PAIR
+    half = features // 2
+    low, wide = jnp.bfloat16, jnp.float32
+    vmem = pl.BlockSpec(memory_space=pltpu.VMEM)
+    anywhere = pl.BlockSpec(memory_space=pl.ANY)
+    dma = pltpu.SemaphoreType.DMA
+    tiny_slots = n_tp + outer + PAIR
     factor = jnp.stack([left_factor.T, right_factor.T])
-    factors, dirs, first_new, second_new, squares = moment_kernel(
-        n_fs,
-        n_tp,
+    return pl.pallas_call(
+        functools.partial(kernel, n_fs, n_tp),
+        out_shape=(
+            jax.ShapeDtypeStruct((width, features), wide),
+            jax.ShapeDtypeStruct((features, width), wide),
+            jax.ShapeDtypeStruct((model, features), low),
+            jax.ShapeDtypeStruct((features, model), low),
+            jax.ShapeDtypeStruct(first_moment.shape, wide),
+            jax.ShapeDtypeStruct(first_moment.shape, wide),
+        ),
+        in_specs=[anywhere] * 6 + [vmem] * 3,
+        out_specs=(vmem,) * 6,
+        scratch_shapes=[
+            pltpu.VMEM((2, rank, model), low),
+            pltpu.VMEM((2, rank, features), low),
+            pltpu.VMEM((width, features), wide),
+            pltpu.VMEM((features, width), wide),
+            pltpu.VMEM((width, half), low),
+            pltpu.VMEM((half, width), low),
+            pltpu.VMEM((tokens, model), low),
+            pltpu.VMEM((tokens, model), low),
+            pltpu.VMEM((tokens, features), low),
+            pltpu.VMEM((tokens, features), low),
+            pltpu.VMEM((2, rank, tokens), low),
+            pltpu.VMEM((2, rank, features), wide),
+            pltpu.VMEM((outer, 2, depth, features), low),
+            pltpu.VMEM((outer, 2, depth, features), low),
+            pltpu.VMEM((outer, 2, depth, features), low),
+            pltpu.VMEM((outer, 2, depth, features), low),
+            pltpu.VMEM((2, depth, features), low),
+            pltpu.VMEM((tiny_slots, 8, 128), wide),
+            dma((6,)),
+            dma((2, 2, outer)),
+            dma((2, 2, 2, n_tp // PAIR)),
+            dma((2, 2, n_tp // PAIR)),
+            dma((2, outer)),
+            dma((2, outer)),
+            dma((2, 2, outer)),
+            dma((2, tiny_slots)),
+            dma((2, 2, 2, outer)),
+            dma((2, 2, 2, outer)),
+        ],
+        compiler_params=pltpu.CompilerParams(
+            collective_id=0, has_side_effects=True, vmem_limit_bytes=56 * 2**20
+        ),
+        cost_estimate=pl.CostEstimate(
+            flops=4 * tokens * rank * (model + features), bytes_accessed=200 * 2**20, transcendentals=0
+        ),
+    )(
         saved_inputs,
         out_cotangent,
         query_cotangent,
         attn_outputs,
+        query_master,
+        out_master,
         factor,
         first_moment,
         second_moment,
     )
-    rank, features = dirs.shape[1:]
-    entries = rank * features * n_tp
-    scale = 0.01 * lax.rsqrt(squares[:2, 0] / entries + 1e-06)
-    width = left_factor.shape[0]
-    start = lax.axis_index("fs") * width
-    own = lax.dynamic_slice_in_dim(factors, start, width, axis=2)
-    f32 = jnp.float32
-    query_new = query_master - scale[0] * lax.dot_general(own[0], dirs[0], TN, preferred_element_type=f32)
-    out_new = out_master - scale[1] * lax.dot_general(dirs[1], own[1], TN, preferred_element_type=f32)
-    query_step = lax.dot_general(factors[0], dirs[0], TN, preferred_element_type=f32)
-    out_step = lax.dot_general(dirs[1], factors[1], TN, preferred_element_type=f32)
-    query_copy = (query_all.astype(f32) * (1 / MASTER_GAIN) - scale[0] * query_step).astype(jnp.bfloat16)
-    out_copy = (out_all.astype(f32) * (1 / MASTER_GAIN) - scale[1] * out_step).astype(jnp.bfloat16)
-    return (query_new, out_new, query_copy, out_copy, first_new, second_new)
 
 
 def plain_body(
@@ -425,9 +492,9 @@
 
 def choose_body(n_fs, n_tp, *args):
     left_factor, first_moment = args[4], args[8]
-    model, part = left_factor.shape
-    aligned = model % 128 == 0 and part % 16 == 0 and first_moment.shape[1] % 16 == 0
-    aligned = aligned and first_moment.shape[2] % 128 == 0
+    model, part = args[0].shape[1], left_factor.shape[1]
+    aligned = part % 16 == 0 and first_moment.shape[1] % 16 == 0
+    aligned = aligned and model // n_fs % 128 == 0 and first_moment.shape[2] % 256 == 0
     if aligned and n_fs % PAIR == 0 and n_tp % PAIR == 0:
         return fast_body(n_fs, n_tp, *args)
     return plain_body(*args)

time: 299 us -> 195 us (0.65)
  blocking collectives: 189 us -> 0 us
  Pallas kernels: 85.4 us -> 182 us
  matrix products: 17.5 us -> 0 us
  local copies, waits for them, and re-layouts: 1.97 us -> 10.8 us
    all_gather x2 -> x0, blocking collectives: 189 us -> none  [the longest x1 96.4 us: fast_body(): lax.all_gather((out_master * MASTER_GAIN).astype(jnp.float16), 'fs', axis...]
    pallas_call x1, Pallas kernels: 85.4 us -> 182 us  [fast_body(): pl.pallas_call(functools.partial(kernel, n_fs, n_tp), out_shape=(jax.Shap...]
    dot_general x4 -> x0, matrix products: 17.5 us -> none  [the longest x1 7.56 us: fast_body(): lax.dot_general(dirs[1], factors[1], TN, preferred_element_type=f32)]
    unnamed x16, local copies, waits for them, and re-layouts: 1.45 us -> 10.8 us
where the time goes in v2:
time: 195 us
  Pallas kernels  182 us (93%)
  local copies, waits for them, and re-layouts  10.8 us (6%)
    pallas_call x1, Pallas kernels, fast_body(): pl.pallas_call(functools.partial(kernel, n_fs, n_tp), out_shape=(jax.Shap...  182 us
    unnamed x16, local copies, waits for them, and re-layouts  10.8 us

profile of v2, /device:TPU:0, one launch (start us, length us, event | category | flops | bytes accessed | tf_op | source)
XLA Modules:
  0.0 195.1 jit_solution(17375287755987244567)
XLA Ops:
  0.6 1.6 pad_maximum_fusion.factor_ref
  2.2 182.0 %shard_map.145 = (f32[384,768]{1,0:T(8,128)}, f32[768,384]{1,0:T(8,128)}, bf16[3072,768]{1,0:T(8,128)(2,1)}, bf16[768,3072]{1,0:T(8,128)(2,1)}, f32[2,48,768]{2,1,0:T(8,128)}, /*index=5*/f32[2,48,768]{2,1,0:T(8,128)}) custom-call(bf16[512,3072]{1,0:T(8,128)(2,1)} %saved_hbm.1, bf16[512,3072]{1,0:T(8,128)(2,1)} %outcot_hbm.1, bf16[512,768]{1,0:T(8,128)(2,1)} %querycot_hbm.1, ...), custom_call_target="tpu_custom_call" | custom-call | flops 3019898880 | bytes 209715200 | tf_op jit(solution)/shard_map/pallas_call | solution.py:378
  184.3 0.0 copy-start
  184.3 2.5 %copy.22 = f32[384,768]{1,0:T(8,128)} copy(f32[384,768]{1,0:T(8,128)} %get-tuple-element.12) | data formatting | bytes 2359296
  186.8 0.0 slice-start
  186.8 2.5 %copy.23 = f32[768,384]{1,0:T(8,128)} copy(f32[768,384]{1,0:T(8,128)} %get-tuple-element.13) | data formatting | bytes 2359296
  189.3 0.0 copy-done
  189.3 0.0 slice-start.1
  189.3 2.2 %copy.24 = bf16[3072,768]{1,0:T(8,128)(2,1)} copy(bf16[3072,768]{1,0:T(8,128)(2,1)S(1)} %copy-done) | data formatting | bytes 9437184
  191.5 0.0 slice-done
  191.5 0.0 slice-done.1
  191.5 0.0 copy-start.2
  191.5 0.0 copy-start.1
  191.5 2.2 %copy.25 = bf16[768,3072]{1,0:T(8,128)(2,1)} copy(bf16[768,3072]{1,0:T(8,128)(2,1)S(1)} %bitcast.7) | data formatting | bytes 9437184
  193.7 0.0 copy-done.2
  193.7 0.7 copy.26
  194.4 0.0 copy-done.1
  194.4 0.7 copy.27
  (1 shorter events, 0.0 us)
Async XLA Ops:
  184.3 5.0 %copy-start = (bf16[3072,768]{1,0:T(8,128)(2,1)S(1)}, bf16[3072,768]{1,0:T(8,128)(2,1)}, u32[]{:S(2)}) copy-start(bf16[3072,768]{1,0:T(8,128)(2,1)} %get-tuple-element.14) | copy-start | bytes 14155780
  186.8 4.7 %slice-start = ((s8[4718592]{0:T(1024)(128)(4,1)}), s8[4194304]{0:T(1024)(128)(4,1)S(1)}, s32[]{:S(2)}) async-start(s8[4718592]{0:T(1024)(128)(4,1)} %bitcast.6), calls=%async_computation | async-start | bytes 8388608
  189.3 2.2 %slice-start.1 = ((s8[4718592]{0:T(1024)(128)(4,1)}), s8[524288]{0:T(1024)(128)(4,1)S(1)}, s32[]{:S(2)}) async-start(s8[4718592]{0:T(1024)(128)(4,1)} %bitcast.6), calls=%async_computation.1 | async-start | bytes 1048576
  191.5 2.2 %copy-start.2 = (f32[2,48,768]{2,1,0:T(8,128)S(1)}, f32[2,48,768]{2,1,0:T(8,128)}, u32[]{:S(2)}) copy-start(f32[2,48,768]{2,1,0:T(8,128)} %get-tuple-element.16) | copy-start | bytes 884740
  191.5 2.9 %copy-start.1 = (f32[2,48,768]{2,1,0:T(8,128)S(1)}, f32[2,48,768]{2,1,0:T(8,128)}, u32[]{:S(2)}) copy-start(f32[2,48,768]{2,1,0:T(8,128)} %get-tuple-element.17) | copy-start | bytes 884740

commit v3 on v2

--- a/solution.py
+++ b/solution.py
@@ -308,21 +308,34 @@
         pair = (factor, direction) if k == 0 else (direction, factor)
         return lax.dot_general(*pair, TN, preferred_element_type=jnp.float32)
 
-    late = (
-        Gather("fs", n_fs, lambda i: query_copy.at[rows(i, width), half:], late_sems.at[0]),
-        Gather("fs", n_fs, lambda i: out_copy.at[half:, rows(i, width)], late_sems.at[1]),
-    )
+    tall, deep = width // 2, half // 2
+    late_query = [
+        Gather("fs", n_fs, lambda i, p=p: query_copy.at[rows(2 * i + p, tall), half:], late_sems.at[p])
+        for p in range(2)
+    ]
+    late_out = [
+        Gather(
+            "fs",
+            n_fs,
+            lambda i, p=p: out_copy.at[half + p * deep : half + (p + 1) * deep, rows(i, width)],
+            late_sems.at[2 + p],
+        )
+        for p in range(2)
+    ]
+    late = late_query + late_out
     for part_of_features in (slice(half, None), slice(0, half)):
         query_new = query_master[:, part_of_features] - query_scale * step(0, me, part_of_features)
         query_out[:, part_of_features] = query_new
         query_copy[rows(me, width), part_of_features] = query_new.astype(query_copy.dtype)
         if part_of_features.start:
-            late[0].start()
+            for gather in late_query:
+                gather.start()
         out_new = out_master[part_of_features, :] - out_scale * step(1, me, part_of_features)
         out_out[part_of_features, :] = out_new
         out_copy[part_of_features, rows(me, width)] = out_new.astype(out_copy.dtype)
         if part_of_features.start:
-            late[1].start()
+            for gather in late_out:
+                gather.start()
     for gather in early:
         gather.finish()
 
@@ -415,7 +428,7 @@
             dma((2, 2, outer)),
             dma((2, tiny_slots)),
             dma((2, 2, 2, outer)),
-            dma((2, 2, 2, outer)),
+            dma((4, 2, 2, outer)),
         ],
         compiler_params=pltpu.CompilerParams(
             collective_id=0, has_side_effects=True, vmem_limit_bytes=56 * 2**20
@@ -495,6 +508,7 @@
     model, part = args[0].shape[1], left_factor.shape[1]
     aligned = part % 16 == 0 and first_moment.shape[1] % 16 == 0
     aligned = aligned and model // n_fs % 128 == 0 and first_moment.shape[2] % 256 == 0
+    aligned = aligned and model // n_fs % 32 == 0 and first_moment.shape[2] % 64 == 0
     if aligned and n_fs % PAIR == 0 and n_tp % PAIR == 0:
         return fast_body(n_fs, n_tp, *args)
     return plain_body(*args)

time: 195 us -> 195 us (level)
  no operation moved by 1% of the time
where the time goes in v3:
time: 195 us
  Pallas kernels  182 us (93%)
  local copies, waits for them, and re-layouts  10.8 us (6%)
    pallas_call x1, Pallas kernels, fast_body(): pl.pallas_call(functools.partial(kernel, n_fs, n_tp), out_shape=(jax.Shap...  182 us
    unnamed x16, local copies, waits for them, and re-layouts  10.8 us

profile of v3, /device:TPU:0, one launch (start us, length us, event | category | flops | bytes accessed | tf_op | source)
XLA Modules:
  0.0 194.7 jit_solution(6283920057721334857)
XLA Ops:
  0.6 1.6 pad_maximum_fusion.factor_ref
  2.2 181.6 %shard_map.145 = (f32[384,768]{1,0:T(8,128)}, f32[768,384]{1,0:T(8,128)}, bf16[3072,768]{1,0:T(8,128)(2,1)}, bf16[768,3072]{1,0:T(8,128)(2,1)}, f32[2,48,768]{2,1,0:T(8,128)}, /*index=5*/f32[2,48,768]{2,1,0:T(8,128)}) custom-call(bf16[512,3072]{1,0:T(8,128)(2,1)} %saved_hbm.1, bf16[512,3072]{1,0:T(8,128)(2,1)} %outcot_hbm.1, bf16[512,768]{1,0:T(8,128)(2,1)} %querycot_hbm.1, ...), custom_call_target="tpu_custom_call" | custom-call | flops 3019898880 | bytes 209715200 | tf_op jit(solution)/shard_map/pallas_call | solution.py:391
  183.9 0.0 copy-start
  183.9 2.5 %copy.22 = f32[384,768]{1,0:T(8,128)} copy(f32[384,768]{1,0:T(8,128)} %get-tuple-element.12) | data formatting | bytes 2359296
  186.4 0.0 slice-start
  186.4 2.5 %copy.23 = f32[768,384]{1,0:T(8,128)} copy(f32[768,384]{1,0:T(8,128)} %get-tuple-element.13) | data formatting | bytes 2359296
  188.9 0.0 copy-done
  188.9 0.0 slice-start.1
  188.9 2.2 %copy.24 = bf16[3072,768]{1,0:T(8,128)(2,1)} copy(bf16[3072,768]{1,0:T(8,128)(2,1)S(1)} %copy-done) | data formatting | bytes 9437184
  191.1 0.0 slice-done
  191.1 0.0 slice-done.1
  191.1 0.0 copy-start.2
  191.1 0.0 copy-start.1
  191.1 2.2 %copy.25 = bf16[768,3072]{1,0:T(8,128)(2,1)} copy(bf16[768,3072]{1,0:T(8,128)(2,1)S(1)} %bitcast.7) | data formatting | bytes 9437184
  193.3 0.0 copy-done.2
  193.3 0.7 copy.26
  194.0 0.0 copy-done.1
  194.0 0.7 copy.27
  (1 shorter events, 0.0 us)
Async XLA Ops:
  183.9 5.0 %copy-start = (bf16[3072,768]{1,0:T(8,128)(2,1)S(1)}, bf16[3072,768]{1,0:T(8,128)(2,1)}, u32[]{:S(2)}) copy-start(bf16[3072,768]{1,0:T(8,128)(2,1)} %get-tuple-element.14) | copy-start | bytes 14155780
  186.4 4.7 %slice-start = ((s8[4718592]{0:T(1024)(128)(4,1)}), s8[4194304]{0:T(1024)(128)(4,1)S(1)}, s32[]{:S(2)}) async-start(s8[4718592]{0:T(1024)(128)(4,1)} %bitcast.6), calls=%async_computation | async-start | bytes 8388608
  188.9 2.2 %slice-start.1 = ((s8[4718592]{0:T(1024)(128)(4,1)}), s8[524288]{0:T(1024)(128)(4,1)S(1)}, s32[]{:S(2)}) async-start(s8[4718592]{0:T(1024)(128)(4,1)} %bitcast.6), calls=%async_computation.1 | async-start | bytes 1048576
  191.1 2.2 %copy-start.2 = (f32[2,48,768]{2,1,0:T(8,128)S(1)}, f32[2,48,768]{2,1,0:T(8,128)}, u32[]{:S(2)}) copy-start(f32[2,48,768]{2,1,0:T(8,128)} %get-tuple-element.16) | copy-start | bytes 884740
  191.1 2.9 %copy-start.1 = (f32[2,48,768]{2,1,0:T(8,128)S(1)}, f32[2,48,768]{2,1,0:T(8,128)}, u32[]{:S(2)}) copy-start(f32[2,48,768]{2,1,0:T(8,128)} %get-tuple-element.17) | copy-start | bytes 884740
